TPU v7x, 32 devices: a whole 2x2x4 slice. The times are simulated.
32 devices in a mesh: sp: 8 (over z, y), dp: 4 (over x, core).
Axes of the slice: x: 2, y: 2, z: 4, core: 2. Of those that a mesh axis runs over, the one named last changes fastest.
Arguments:
- queries: bfloat16 [4, 1024, 2048], P('dp', 'sp'), may hold values from -40 to 40
- keys: bfloat16 [4, 1024, 512], P('dp', 'sp'), may hold values from -8 to 8
- values: bfloat16 [4, 1024, 512], P('dp', 'sp'), may hold values from -6 to 6
- lambdas: float32 [16], replicated, may hold values from 0.3 to 0.8
- value_gain: float32 [128], replicated, may hold values from 0.1 to 1.9
- out_weight: bfloat16 [2048, 4096], P(None, ('sp', 'dp')), may hold values from -0.125 to 0.125
Outputs:
- mixed: bfloat16 [4, 1024, 4096], P('dp', 'sp')
All inputs are finite; a program needn't handle non-finite values.
Results may differ from a plain program's by a relative error of at most 0.0087.
Values may be sent and summed in bfloat16 or wider, within the bound.
A program may use at most 128 MiB of HBM per device.

v0:
```python
import jax
import jax.numpy as jnp
from jax import lax
from jax.sharding import PartitionSpec as P

HEADS = 16
KV_HEADS = 4
HEAD_DIM = 64
VALUE_DIM = 128
rope_base = 500000.0
output_scale = 0.8
norm_eps = 1e-05


def swapped(block, axis, distance):
    count = lax.axis_size(axis)
    route = []
    for low in range(count):
        high = low | 1 << distance
        if high != low and high < count:
            route += [(low, high), (high, low)]
    return lax.ppermute(block, axis, route)


def rotate(parts, positions):
    width = parts.shape[-1]
    half = width // 2
    freqs = rope_base ** (-jnp.arange(0, width, 2, dtype=jnp.float32) / width)
    angles = positions[:, None] * freqs[None, :]
    shape = (angles.shape[0],) + (1,) * (parts.ndim - 2) + (half,)
    cosine = jnp.cos(angles).reshape(shape)
    sine = jnp.sin(angles).reshape(shape)
    first = parts[..., :half]
    second = parts[..., half:]
    return jnp.concatenate([first * cosine - second * sine, second * cosine + first * sine], -1)


def gather_group(key_value, group_size):
    tok_rows = key_value.shape[0]
    sub_rows = tok_rows // group_size
    width = key_value.shape[-1]
    arranged = key_value.reshape(group_size, sub_rows, KV_HEADS, 2, width)
    arranged = jnp.transpose(arranged, (2, 0, 1, 3, 4)).reshape(
        group_size * KV_HEADS, sub_rows, 2, width
    )
    received = lax.all_to_all(arranged, "sp", split_axis=0, concat_axis=1, tiled=True)
    held = received.reshape(1, -1, sub_rows, 2, width)
    device_index = lax.axis_index("sp")
    for bit_number in range(group_size.bit_length() - 1):
        partner = swapped(held, "sp", bit_number)
        upper = device_index // 2**bit_number % 2 == 1
        held = jnp.concatenate(
            [jnp.where(upper, partner, held), jnp.where(upper, held, partner)], 0
        )
    ordered = jnp.transpose(held, (1, 0, 2, 3, 4)).reshape(-1, 2, width)
    return (ordered[:, 0], ordered[:, 1])


def attend(query_rot, key_rot, value_whole, lambda_heads, value_gain):
    seqlen = key_rot.shape[0]
    block_rows = min(512, seqlen)
    count = seqlen // block_rows
    score_scale = query_rot.shape[-1] ** (-0.5)
    outputs = []
    for block_index in range(count):
        start = block_index * block_rows
        reach = start + block_rows
        query_block = query_rot[start:reach]
        key_part = key_rot[:reach]
        value_part = value_whole[:reach]
        scores = (
            jnp.einsum("qhmd,kmd->hmqk", query_block, key_part, preferred_element_type=jnp.float32)
            * score_scale
        )
        allowed = jnp.arange(reach)[None, :] <= (start + jnp.arange(block_rows))[:, None]
        scores = jnp.where(allowed[None, None], scores, -jnp.inf)
        row_top = jnp.max(scores, -1, keepdims=True)
        raised = jnp.exp(scores - row_top)
        maps = raised / jnp.sum(raised, -1, keepdims=True)
        weights = (maps[:, 0] - lambda_heads[:, None, None] * maps[:, 1]).astype(jnp.bfloat16)
        outputs.append(
            jnp.einsum("hqk,ke->qhe", weights, value_part, preferred_element_type=jnp.float32)
        )
    head_values = jnp.concatenate(outputs, 0)
    squares = jnp.mean(head_values * head_values, -1, keepdims=True)
    normed = head_values * lax.rsqrt(squares + norm_eps) * value_gain * output_scale
    return normed.astype(jnp.bfloat16)


def shards(queries, keys, values, lambdas, value_gain, out_weight):
    tok_rows = queries.shape[1]
    sp_count = lax.axis_size("sp")
    group_size = sp_count // KV_HEADS
    per_device = HEADS // sp_count
    query_split = queries[0].reshape(tok_rows, HEADS, 2 * HEAD_DIM)
    key_split = keys[0].reshape(tok_rows, KV_HEADS, 2 * HEAD_DIM)
    value_split = values[0].reshape(tok_rows, KV_HEADS, VALUE_DIM)
    query_heads = lax.all_to_all(query_split, "sp", split_axis=1, concat_axis=0, tiled=True)
    key_whole, value_whole = gather_group(jnp.stack([key_split, value_split], 2), group_size)
    seqlen = query_heads.shape[0]
    positions = jnp.arange(seqlen, dtype=jnp.float32)
    query_rot = rotate(
        query_heads.reshape(seqlen, per_device, 2, HEAD_DIM).astype(jnp.float32), positions
    ).astype(jnp.bfloat16)
    key_rot = rotate(key_whole.reshape(seqlen, 2, HEAD_DIM).astype(jnp.float32), positions).astype(
        jnp.bfloat16
    )
    lambda_heads = lax.dynamic_slice_in_dim(
        lambdas, lax.axis_index("sp") * per_device, per_device, 0
    )
    head_out = attend(query_rot, key_rot, value_whole, lambda_heads, value_gain)
    heads_local = lax.all_to_all(
        head_out.reshape(seqlen, per_device * VALUE_DIM),
        "sp",
        split_axis=0,
        concat_axis=1,
        tiled=True,
    )
    mixed = jnp.dot(
        heads_local,
        lax.all_gather(out_weight, ("sp", "dp"), axis=1, tiled=True),
        preferred_element_type=jnp.float32,
    ).astype(jnp.bfloat16)
    return mixed[None]


def solution(mesh):
    return jax.shard_map(
        shards,
        mesh=mesh,
        in_specs=(
            P("dp", "sp", None),
            P("dp", "sp", None),
            P("dp", "sp", None),
            P(),
            P(),
            P(None, ("sp", "dp")),
        ),
        out_specs=P("dp", "sp", None),
        check_vma=False,
    )
```

profile of v0, /device:TPU:0, one launch (start us, length us, event | category | flops | bytes accessed | tf_op | source)
XLA Modules:
  0.0 182.8 jit_solution(17417908235289656183)
XLA Ops:
  6.5 0.0 copy-start
  6.5 0.0 copy-start.2
  6.5 0.0 all-gather.2.cloned.1.call-start
  6.5 0.7 all-gather.2.cloned.1.call-update
  7.3 0.9 stack.7
  8.2 0.9 stack.8
  9.2 0.7 pad_maximum_fusion.3
  9.9 7.3 %all-to-all-start = ((bf16[8,64,2,128]{3,1,2,0:T(8,128)(2,1)}), bf16[8,64,2,128]{3,1,2,0:T(8,128)(2,1)S(1)}, u32[]{:S(2)}, u32[]{:S(2)}) async-start(bf16[8,64,2,128]{3,1,2,0:T(8,128)(2,1)} %bitcast.1), calls=%async_computation | async-start | bytes 524288 | tf_op jit(solution)/shard_map/all_to_all | solution.py:46
  17.2 2.0 %copy.40 = bf16[1,128,2048]{1,2,0:T(8,128)(2,1)} copy(bf16[1,128,2048]{2,1,0:T(8,128)(2,1)} %param.6) | data formatting | bytes 1048576 | tf_op args[0]
  19.3 0.5 fusion.39
  19.8 0.4 iota_compare_fusion
  20.2 6.0 %all-to-all-done = bf16[8,64,2,128]{3,1,2,0:T(8,128)(2,1)S(1)} async-done(((bf16[8,64,2,128]{3,1,2,0:T(8,128)(2,1)}), bf16[8,64,2,128]{3,1,2,0:T(8,128)(2,1)S(1)}, u32[]{:S(2)}, u32[]{:S(2)}) %all-to-all-start) | async-done | bytes 262176 | tf_op jit(solution)/shard_map/all_to_all | solution.py:46
  26.3 3.5 %all-to-all-start.1 = ((bf16[128,16,128]{0,2,1:T(8,128)(2,1)}), bf16[128,16,128]{0,2,1:T(8,128)(2,1)S(1)}, u32[]{:S(2)}, u32[]{:S(2)}) async-start(bf16[128,16,128]{0,2,1:T(8,128)(2,1)} %bitcast.10), calls=%async_computation.1 | async-start | bytes 1048576 | tf_op jit(solution)/shard_map/all_to_all | solution.py:98
  29.8 2.0 %collective-permute-start = (bf16[1,8,64,2,128]{4,2,3,1,0:T(8,128)(2,1)S(1)}, bf16[1,8,64,2,128]{4,2,3,1,0:T(8,128)(2,1)S(1)}, u32[]{:S(2)}, u32[]{:S(2)}) collective-permute-start(bf16[1,8,64,2,128]{4,2,3,1,0:T(8,128)(2,1)S(1)} %bitcast.118), channel_id=1, source_target_pairs={{0,4},{4,0},{8,12},{12,8},{16,20},{20,16},{24,28},{28,24},{1,5},{5... | collective-permute-start | bytes 786440 | tf_op jit(solution)/shard_map/ppermute | solution.py:22
  31.8 0.0 copy-done
  31.8 0.8 iota_compare_fusion.1
  32.5 0.0 copy-done.2
  32.5 0.1 dynamic_slice.3
  32.6 13.4 %collective-permute-done = bf16[1,8,64,2,128]{4,2,3,1,0:T(8,128)(2,1)S(1)} collective-permute-done((bf16[1,8,64,2,128]{4,2,3,1,0:T(8,128)(2,1)S(1)}, bf16[1,8,64,2,128]{4,2,3,1,0:T(8,128)(2,1)S(1)}, u32[]{:S(2)}, u32[]{:S(2)}) %collective-permute-start) | collective-permute-done | bytes 262176 | tf_op jit(solution)/shard_map/ppermute | solution.py:22
  46.1 0.1 maximum_bitcast_fusion
  46.2 0.2 copy.39
  46.4 0.7 subtract_convert_fusion.1
  47.2 6.0 %all-to-all-done.1 = bf16[128,16,128]{0,2,1:T(8,128)(2,1)S(1)} async-done(((bf16[128,16,128]{0,2,1:T(8,128)(2,1)}), bf16[128,16,128]{0,2,1:T(8,128)(2,1)S(1)}, u32[]{:S(2)}, u32[]{:S(2)}) %all-to-all-start.1) | async-done | bytes 524320 | tf_op jit(solution)/shard_map/all_to_all | solution.py:98
  53.1 0.1 convert_element_type.55
  53.2 0.6 copy.42
  53.9 0.2 reshape.176
  54.0 0.1 fusion.63
  54.1 0.1 subtract_convert_fusion
  54.3 4.5 %fusion.69 = (f32[2,2,512]{2,0,1:T(2,128)S(1)}, f32[2,2,512,512]{2,3,0,1:T(8,128)}) fusion(pred[512,512]{0,1:T(8,128)(4,1)} %iota_compare_fusion.1, bf16[1024,2,32]{0,2,1:T(8,128)(2,1)S(1)} %get-tuple-element.9, bf16[1024,2,32]{0,2,1:T(8,128)(2,1)} %get-tuple-element.10, bf16[1024,2,2,32]{0,3,1,2:T(8,128)(2,1)S(1)} %get-tuple-element.5, ...), kind=kOutput, calls=%fused_computation.77 | convolution fusion | flops 139198976 | bytes 5251072 | tf_op jit(solution)/shard_map/sub | solution.py:78
  58.8 0.0 copy-start.1
  58.8 3.0 %broadcast_divide_fusion.1 = f32[2,2,512,512]{2,3,0,1:T(8,128)S(1)} fusion(f32[2,2,512,512]{2,3,0,1:T(8,128)} %get-tuple-element.18, f32[2,2,512]{2,0,1:T(2,128)S(1)} %get-tuple-element.17), kind=kLoop, calls=%fused_computation.22 | loop fusion | flops 1048576 | bytes 8396800 | tf_op jit(solution)/shard_map/div | solution.py:79
  61.9 0.4 fusion.19
  62.3 0.0 copy-done.1
  62.3 5.3 %fusion.64 = (f32[2,2,512]{2,0,1:T(2,128)S(1)}, f32[2,2,512,1024]{2,3,0,1:T(8,128)}) fusion(pred[512,1024]{0,1:T(8,128)(4,1)S(1)} %iota_compare_fusion, bf16[1024,2,32]{0,2,1:T(8,128)(2,1)S(1)} %copy-done.1, bf16[1024,2,32]{0,2,1:T(8,128)(2,1)S(1)} %get-tuple-element.9, bf16[1024,2,2,32]{0,3,1,2:T(8,128)(2,1)S(1)} %get-tuple-element.6, ...), kind=kOutput, calls=%fused_computation.76 | convolution fusion | flops 277873664 | bytes 9707520 | tf_op jit(solution)/shard_map/sub | solution.py:78
  67.6 4.5 %broadcast_divide_fusion = f32[2,2,512,1024]{2,3,0,1:T(8,128)S(1)} fusion(f32[2,2,512,1024]{2,3,0,1:T(8,128)} %get-tuple-element.16, f32[2,2,512]{2,0,1:T(2,128)S(1)} %get-tuple-element.15), kind=kLoop, calls=%fused_computation.11 | loop fusion | flops 2097152 | bytes 16785408 | tf_op jit(solution)/shard_map/div | solution.py:79
  72.1 0.6 fusion.15
  72.8 0.1 fusion.21
  72.9 0.1 mul.266
  73.0 0.2 copy.61
  73.2 0.4 copy.50
  73.6 0.2 copy.48
  73.8 0.2 copy.49
  74.0 0.1 pad_maximum_fusion
  74.1 0.2 multiply_convert_fusion
  74.3 32.6 %all_to_all.34 = bf16[8,128,256]{2,1,0:T(8,128)(2,1)S(1)} all-to-all(bf16[8,128,256]{2,1,0:T(8,128)(2,1)S(1)} %multiply_convert_fusion), channel_id=1, replica_groups=mesh['sp'=8,'dp'=4] {'sp'}, dimensions={0} | all-to-all | bytes 1048576 | tf_op jit(solution)/shard_map/all_to_all | solution.py:112
  106.9 0.3 copy.51
  107.2 59.7 %all-gather.2.cloned.1.call-done = bf16[2048,4096]{1,0:T(8,128)(2,1)} async-done(((bf16[2048,128]{1,0:T(8,128)(2,1)}), bf16[2048,4096]{1,0:T(8,128)(2,1)}) %all-gather.2.cloned.1.call-update) | async-done | bytes 16777232 | tf_op jit(solution)/shard_map/all_gather | solution.py:121
  166.8 9.1 %fusion.3 = bf16[1,128,4096]{2,1,0:T(8,128)(2,1)} fusion(bf16[128,2048]{0,1:T(8,128)(2,1)S(1)} %bitcast.112, bf16[2048,4096]{1,0:T(8,128)(2,1)} %all-gather.2.cloned.1.call-done), kind=kOutput, calls=%fused_computation.6 | convolution fusion | flops 2148007936 | bytes 18350080 | tf_op jit(solution)/shard_map/dot_general | solution.py:119
  (9 shorter events, 0.2 us)
Async XLA Ops:
  6.5 25.2 %copy-start = (f32[128]{0:T(128)S(1)}, f32[128]{0:T(128)}, u32[]{:S(2)}) copy-start(f32[128]{0:T(128)} %param.10) | copy-start | bytes 1540
  6.5 26.0 %copy-start.2 = (f32[16]{0:T(128)S(1)}, f32[16]{0:T(128)}, u32[]{:S(2)}) copy-start(f32[16]{0:T(128)} %param.9) | copy-start | bytes 196
  6.5 160.3 %all-gather.2.cloned.1.call-start = ((), (), s32[]{:S(2)}) async-start(), calls=%async_computation.3 | async-start | bytes 17301504 | tf_op jit(solution)/shard_map/all_gather | solution.py:121
  9.9 16.3 %all-to-all-start = ((bf16[8,64,2,128]{3,1,2,0:T(8,128)(2,1)}), bf16[8,64,2,128]{3,1,2,0:T(8,128)(2,1)S(1)}, u32[]{:S(2)}, u32[]{:S(2)}) async-start(bf16[8,64,2,128]{3,1,2,0:T(8,128)(2,1)} %bitcast.1), calls=%async_computation | async-start | bytes 524288 | tf_op jit(solution)/shard_map/all_to_all | solution.py:46
  26.3 26.9 %all-to-all-start.1 = ((bf16[128,16,128]{0,2,1:T(8,128)(2,1)}), bf16[128,16,128]{0,2,1:T(8,128)(2,1)S(1)}, u32[]{:S(2)}, u32[]{:S(2)}) async-start(bf16[128,16,128]{0,2,1:T(8,128)(2,1)} %bitcast.10), calls=%async_computation.1 | async-start | bytes 1048576 | tf_op jit(solution)/shard_map/all_to_all | solution.py:98
  29.8 16.3 %collective-permute-start = (bf16[1,8,64,2,128]{4,2,3,1,0:T(8,128)(2,1)S(1)}, bf16[1,8,64,2,128]{4,2,3,1,0:T(8,128)(2,1)S(1)}, u32[]{:S(2)}, u32[]{:S(2)}) collective-permute-start(bf16[1,8,64,2,128]{4,2,3,1,0:T(8,128)(2,1)S(1)} %bitcast.118), channel_id=1, source_target_pairs={{0,4},{4,0},{8,12},{12,8},{16,20},{20,16},{24,28},{28,24},{1,5},{5... | collective-permute-start | bytes 786440 | tf_op jit(solution)/shard_map/ppermute | solution.py:22
  58.8 3.5 %copy-start.1 = (bf16[1024,2,32]{0,2,1:T(8,128)(2,1)S(1)}, bf16[1024,2,32]{0,2,1:T(8,128)(2,1)}, u32[]{:S(2)}) copy-start(bf16[1024,2,32]{0,2,1:T(8,128)(2,1)} %get-tuple-element.10) | copy-start | bytes 393220
Sparse Core Ops, SparseCore 0:
  10.2 156.6 all-gather.1
where the time goes:
time: 183 us
  waiting for transfers between devices  85.8 us (47%)
  blocking collectives  32.6 us (18%)
  matrix products  20.1 us (11%)
  between operations  13.6 us (7%)
  starting transfers between devices  12.8 us (7%)
  other arithmetic  11.4 us (6%)
  local copies, waits for them, and re-layouts  6.52 us (4%)
    all_gather x1, waiting for transfers between devices, shards(): lax.all_gather(out_weight, ('sp', 'dp'), axis=1, tiled=True)  59.7 us
    all_to_all x1, blocking collectives, shards(): lax.all_to_all(head_out.reshape(seqlen, per_device * VALUE_DIM), 'sp', sp...  32.6 us
    ppermute x1, waiting for transfers between devices, swapped(): return lax.ppermute(block, axis, route)  13.4 us
    sub x2, matrix products, attend(): raised = jnp.exp(scores - row_top)  9.88 us
    dot_general x1, matrix products, shards(): jnp.dot(heads_local, lax.all_gather(out_weight, ('sp', 'dp'), axis=1, til...  9.12 us
    div x2, other arithmetic, attend(): maps = raised / jnp.sum(raised, -1, keepdims=True)  7.49 us
    all_to_all x1, starting transfers between devices, gather_group(): lax.all_to_all(arranged, 'sp', split_axis=0, concat_axis=1, tiled=True)  7.31 us
    all_to_all x1, waiting for transfers between devices, gather_group(): lax.all_to_all(arranged, 'sp', split_axis=0, concat_axis=1, tiled=True)  6.03 us
  transfers between devices with their start and end apart: 4, of which 4 were waited for; matrix products, arithmetic and copies ran while one was open for 16% of the time, Pallas kernels for 0%

commit v1 on v0

--- a/solution.py
+++ b/solution.py
@@ -10,6 +10,11 @@
 rope_base = 500000.0
 output_scale = 0.8
 norm_eps = 1e-05
+
+
+def gather_blocks(x, mesh_axis, dim):
+    tiles = lax.all_gather(x, mesh_axis)
+    return jnp.concatenate(tiles, axis=dim)
 
 
 def swapped(block, axis, distance):
@@ -117,9 +122,7 @@
         tiled=True,
     )
     mixed = jnp.dot(
-        heads_local,
-        lax.all_gather(out_weight, ("sp", "dp"), axis=1, tiled=True),
-        preferred_element_type=jnp.float32,
+        heads_local, gather_blocks(out_weight, ("sp", "dp"), 1), preferred_element_type=jnp.float32
     ).astype(jnp.bfloat16)
     return mixed[None]
 

time: 183 us -> 177 us (0.967)
  waiting for transfers between devices: 85.8 us -> 56.4 us
  local copies, waits for them, and re-layouts: 6.52 us -> 27.9 us
  matrix products: 20.1 us -> 23.4 us
  blocking collectives: 32.6 us -> 29.4 us
    all_gather x1, waiting for transfers between devices: 59.7 us -> 35.9 us  [gather_blocks(): tiles = lax.all_gather(x, mesh_axis)]
    reshape x0 -> x1, local copies, waits for them, and re-layouts: none -> 21.4 us  [gather_blocks(): return jnp.concatenate(tiles, axis=dim)]
    ppermute x1, waiting for transfers between devices: 13.4 us -> 5.86 us  [swapped(): return lax.ppermute(block, axis, route)]
    dot_general x1, matrix products: 9.12 us -> 12.5 us  [shards(): jnp.dot(heads_local, gather_blocks(out_weight, ('sp', 'dp'), 1), preferre...]
    all_to_all x1, blocking collectives: 32.6 us -> 29.4 us  [shards(): lax.all_to_all(head_out.reshape(seqlen, per_device * VALUE_DIM), 'sp', sp...]
where the time goes in v1:
time: 177 us; the launch traced here: 176 us
  waiting for transfers between devices  56.4 us (32%)
  blocking collectives  29.4 us (17%)
  local copies, waits for them, and re-layouts  27.9 us (16%)
  matrix products  23.4 us (13%)
  starting transfers between devices  13.9 us (8%)
  between operations  13.6 us (8%)
  other arithmetic  11.4 us (6%)
    all_gather x1, waiting for transfers between devices, gather_blocks(): tiles = lax.all_gather(x, mesh_axis)  35.9 us
    all_to_all x1, blocking collectives, shards(): lax.all_to_all(head_out.reshape(seqlen, per_device * VALUE_DIM), 'sp', sp...  29.4 us
    reshape x1, local copies, waits for them, and re-layouts, gather_blocks(): return jnp.concatenate(tiles, axis=dim)  21.4 us
    dot_general x1, matrix products, shards(): jnp.dot(heads_local, gather_blocks(out_weight, ('sp', 'dp'), 1), preferre...  12.5 us
    sub x2, matrix products, attend(): raised = jnp.exp(scores - row_top)  9.87 us
    div x2, other arithmetic, attend(): maps = raised / jnp.sum(raised, -1, keepdims=True)  7.5 us
    all_to_all x1, waiting for transfers between devices, gather_group(): lax.all_to_all(arranged, 'sp', split_axis=0, concat_axis=1, tiled=True)  7.43 us
    all_to_all x1, starting transfers between devices, gather_group(): lax.all_to_all(arranged, 'sp', split_axis=0, concat_axis=1, tiled=True)  7.31 us
  transfers between devices with their start and end apart: 4, of which 4 were waited for; matrix products, arithmetic and copies ran while one was open for 16% of the time, Pallas kernels for 0%

profile of v1, /device:TPU:0, one launch (start us, length us, event | category | flops | bytes accessed | tf_op | source)
XLA Modules:
  0.0 176.1 jit_solution(14576190459636888510)
XLA Ops:
  6.5 0.0 copy-start
  6.5 0.0 all-gather.3.cloned.1.call-start
  6.5 0.7 all-gather.3.cloned.1.call-update
  7.3 0.9 stack.7
  8.2 0.9 stack.8
  9.2 0.7 pad_maximum_fusion.3
  9.9 7.3 %all-to-all-start = ((bf16[8,64,2,128]{3,1,2,0:T(8,128)(2,1)}), bf16[8,64,2,128]{3,1,2,0:T(8,128)(2,1)S(1)}, u32[]{:S(2)}, u32[]{:S(2)}) async-start(bf16[8,64,2,128]{3,1,2,0:T(8,128)(2,1)} %bitcast.1), calls=%async_computation | async-start | bytes 524288 | tf_op jit(solution)/shard_map/all_to_all | solution.py:51
  17.2 2.0 %copy.41 = bf16[1,128,2048]{1,2,0:T(8,128)(2,1)} copy(bf16[1,128,2048]{2,1,0:T(8,128)(2,1)} %param.6) | data formatting | bytes 1048576 | tf_op args[0]
  19.3 0.5 fusion.39
  19.8 0.4 iota_compare_fusion
  20.2 7.4 %all-to-all-done = bf16[8,64,2,128]{3,1,2,0:T(8,128)(2,1)S(1)} async-done(((bf16[8,64,2,128]{3,1,2,0:T(8,128)(2,1)}), bf16[8,64,2,128]{3,1,2,0:T(8,128)(2,1)S(1)}, u32[]{:S(2)}, u32[]{:S(2)}) %all-to-all-start) | async-done | bytes 262176 | tf_op jit(solution)/shard_map/all_to_all | solution.py:51
  27.7 4.6 %all-to-all-start.1 = ((bf16[128,16,128]{0,2,1:T(8,128)(2,1)}), bf16[128,16,128]{0,2,1:T(8,128)(2,1)S(1)}, u32[]{:S(2)}, u32[]{:S(2)}) async-start(bf16[128,16,128]{0,2,1:T(8,128)(2,1)} %bitcast.10), calls=%async_computation.1 | async-start | bytes 1048576 | tf_op jit(solution)/shard_map/all_to_all | solution.py:103
  32.2 2.0 %collective-permute-start = (bf16[1,8,64,2,128]{4,2,3,1,0:T(8,128)(2,1)S(1)}, bf16[1,8,64,2,128]{4,2,3,1,0:T(8,128)(2,1)S(1)}, u32[]{:S(2)}, u32[]{:S(2)}) collective-permute-start(bf16[1,8,64,2,128]{4,2,3,1,0:T(8,128)(2,1)S(1)} %bitcast.124), channel_id=1, source_target_pairs={{0,4},{4,0},{8,12},{12,8},{16,20},{20,16},{24,28},{28,24},{1,5},{5... | collective-permute-start | bytes 786440 | tf_op jit(solution)/shard_map/ppermute | solution.py:27
  34.3 0.0 copy-done
  34.3 0.8 iota_compare_fusion.1
  35.0 0.0 copy-done.3
  35.0 0.1 dynamic_slice.3
  35.1 5.9 %collective-permute-done = bf16[1,8,64,2,128]{4,2,3,1,0:T(8,128)(2,1)S(1)} collective-permute-done((bf16[1,8,64,2,128]{4,2,3,1,0:T(8,128)(2,1)S(1)}, bf16[1,8,64,2,128]{4,2,3,1,0:T(8,128)(2,1)S(1)}, u32[]{:S(2)}, u32[]{:S(2)}) %collective-permute-start) | collective-permute-done | bytes 262176 | tf_op jit(solution)/shard_map/ppermute | solution.py:27
  41.0 0.1 maximum_bitcast_fusion
  41.2 0.2 copy.40
  41.4 0.7 subtract_convert_fusion.1
  42.1 6.5 %all-to-all-done.1 = bf16[128,16,128]{0,2,1:T(8,128)(2,1)S(1)} async-done(((bf16[128,16,128]{0,2,1:T(8,128)(2,1)}), bf16[128,16,128]{0,2,1:T(8,128)(2,1)S(1)}, u32[]{:S(2)}, u32[]{:S(2)}) %all-to-all-start.1) | async-done | bytes 524320 | tf_op jit(solution)/shard_map/all_to_all | solution.py:103
  48.6 0.1 convert_element_type.55
  48.7 0.6 copy.43
  49.3 0.2 reshape.184
  49.5 0.1 fusion.63
  49.6 0.1 subtract_convert_fusion
  49.7 4.5 %fusion.69 = (f32[2,2,512]{2,0,1:T(2,128)S(1)}, f32[2,2,512,512]{2,3,0,1:T(8,128)}) fusion(pred[512,512]{0,1:T(8,128)(4,1)} %iota_compare_fusion.1, bf16[1024,2,32]{0,2,1:T(8,128)(2,1)S(1)} %get-tuple-element.9, bf16[1024,2,32]{0,2,1:T(8,128)(2,1)} %get-tuple-element.10, bf16[1024,2,2,32]{0,3,1,2:T(8,128)(2,1)S(1)} %get-tuple-element.5, ...), kind=kOutput, calls=%fused_computation.77 | convolution fusion | flops 139198976 | bytes 5251072 | tf_op jit(solution)/shard_map/sub | solution.py:83
  54.3 3.0 %broadcast_divide_fusion.1 = f32[2,2,512,512]{2,3,0,1:T(8,128)S(1)} fusion(f32[2,2,512,512]{2,3,0,1:T(8,128)} %get-tuple-element.18, f32[2,2,512]{2,0,1:T(2,128)S(1)} %get-tuple-element.17), kind=kLoop, calls=%fused_computation.22 | loop fusion | flops 1048576 | bytes 8396800 | tf_op jit(solution)/shard_map/div | solution.py:84
  57.3 0.4 fusion.19
  57.7 0.0 copy-done.2
  57.8 5.3 %fusion.64 = (f32[2,2,512]{2,0,1:T(2,128)S(1)}, f32[2,2,512,1024]{2,3,0,1:T(8,128)}) fusion(pred[512,1024]{0,1:T(8,128)(4,1)S(1)} %iota_compare_fusion, bf16[1024,2,32]{0,2,1:T(8,128)(2,1)S(1)} %copy-done.2, bf16[1024,2,32]{0,2,1:T(8,128)(2,1)S(1)} %get-tuple-element.9, bf16[1024,2,2,32]{0,3,1,2:T(8,128)(2,1)S(1)} %get-tuple-element.6, ...), kind=kOutput, calls=%fused_computation.76 | convolution fusion | flops 277873664 | bytes 9707520 | tf_op jit(solution)/shard_map/sub | solution.py:83
  63.1 4.5 %broadcast_divide_fusion = f32[2,2,512,1024]{2,3,0,1:T(8,128)S(1)} fusion(f32[2,2,512,1024]{2,3,0,1:T(8,128)} %get-tuple-element.16, f32[2,2,512]{2,0,1:T(2,128)S(1)} %get-tuple-element.15), kind=kLoop, calls=%fused_computation.11 | loop fusion | flops 2097152 | bytes 16785408 | tf_op jit(solution)/shard_map/div | solution.py:84
  67.6 0.6 fusion.15
  68.2 0.1 fusion.21
  68.3 0.1 mul.266
  68.4 0.2 copy.63
  68.6 0.4 copy.51
  69.0 0.2 copy.49
  69.2 0.2 copy.50
  69.4 0.1 pad_maximum_fusion
  69.5 0.2 multiply_convert_fusion
  69.7 29.4 %all_to_all.34 = bf16[8,128,256]{2,1,0:T(8,128)(2,1)S(1)} all-to-all(bf16[8,128,256]{2,1,0:T(8,128)(2,1)S(1)} %multiply_convert_fusion), channel_id=1, replica_groups=mesh['sp'=8,'dp'=4] {'sp'}, dimensions={0} | all-to-all | bytes 1048576 | tf_op jit(solution)/shard_map/all_to_all | solution.py:117
  99.1 0.3 copy.52
  99.4 35.9 %all-gather.3.cloned.1.call-done = bf16[65536,128]{1,0:T(8,128)(2,1)} async-done(((bf16[2048,128]{1,0:T(8,128)(2,1)}), bf16[65536,128]{1,0:T(8,128)(2,1)}) %all-gather.3.cloned.1.call-update) | async-done | bytes 16777232 | tf_op jit(solution)/shard_map/all_gather | solution.py:16
  135.3 21.4 %copy.53 = bf16[2048,32,128]{0,2,1:T(8,128)(2,1)} copy(bf16[2048,32,128]{2,0,1:T(8,128)(2,1)} %bitcast.109) | data formatting | bytes 33554432 | tf_op jit(solution)/shard_map/reshape | solution.py:17
  156.7 12.5 %fusion.3 = bf16[1,128,4096]{2,1,0:T(8,128)(2,1)} fusion(bf16[128,2048]{0,1:T(8,128)(2,1)S(1)} %bitcast.121, bf16[2048,4096]{0,1:T(8,128)(2,1)} %bitcast.108), kind=kOutput, calls=%fused_computation.6 | convolution fusion | flops 2148007936 | bytes 18350080 | tf_op jit(solution)/shard_map/dot_general | solution.py:124
  169.2 0.0 copy-done.1
  (12 shorter events, 0.2 us)
Async XLA Ops:
  6.5 27.7 %copy-start = (f32[128]{0:T(128)S(1)}, f32[128]{0:T(128)}, u32[]{:S(2)}) copy-start(f32[128]{0:T(128)} %param.10) | copy-start | bytes 1540
  6.5 28.5 %copy-start.3 = (f32[16]{0:T(128)S(1)}, f32[16]{0:T(128)}, u32[]{:S(2)}) copy-start(f32[16]{0:T(128)} %param.9) | copy-start | bytes 196
  6.5 128.8 %all-gather.3.cloned.1.call-start = ((), (), s32[]{:S(2)}) async-start(), calls=%async_computation.3 | async-start | bytes 17301504 | tf_op jit(solution)/shard_map/all_gather | solution.py:16
  9.9 17.7 %all-to-all-start = ((bf16[8,64,2,128]{3,1,2,0:T(8,128)(2,1)}), bf16[8,64,2,128]{3,1,2,0:T(8,128)(2,1)S(1)}, u32[]{:S(2)}, u32[]{:S(2)}) async-start(bf16[8,64,2,128]{3,1,2,0:T(8,128)(2,1)} %bitcast.1), calls=%async_computation | async-start | bytes 524288 | tf_op jit(solution)/shard_map/all_to_all | solution.py:51
  27.7 20.9 %all-to-all-start.1 = ((bf16[128,16,128]{0,2,1:T(8,128)(2,1)}), bf16[128,16,128]{0,2,1:T(8,128)(2,1)S(1)}, u32[]{:S(2)}, u32[]{:S(2)}) async-start(bf16[128,16,128]{0,2,1:T(8,128)(2,1)} %bitcast.10), calls=%async_computation.1 | async-start | bytes 1048576 | tf_op jit(solution)/shard_map/all_to_all | solution.py:103
  32.2 8.7 %collective-permute-start = (bf16[1,8,64,2,128]{4,2,3,1,0:T(8,128)(2,1)S(1)}, bf16[1,8,64,2,128]{4,2,3,1,0:T(8,128)(2,1)S(1)}, u32[]{:S(2)}, u32[]{:S(2)}) collective-permute-start(bf16[1,8,64,2,128]{4,2,3,1,0:T(8,128)(2,1)S(1)} %bitcast.124), channel_id=1, source_target_pairs={{0,4},{4,0},{8,12},{12,8},{16,20},{20,16},{24,28},{28,24},{1,5},{5... | collective-permute-start | bytes 786440 | tf_op jit(solution)/shard_map/ppermute | solution.py:27
  54.3 3.5 %copy-start.2 = (bf16[1024,2,32]{0,2,1:T(8,128)(2,1)S(1)}, bf16[1024,2,32]{0,2,1:T(8,128)(2,1)}, u32[]{:S(2)}) copy-start(bf16[1024,2,32]{0,2,1:T(8,128)(2,1)} %get-tuple-element.10) | copy-start | bytes 393220
  156.7 12.5 %copy-start.1 = (f32[128]{0:T(128)S(1)}, f32[128]{0:T(128)}, u32[]{:S(2)}) copy-start(f32[128]{0:T(128)} %param.10) | copy-start | bytes 1540
Sparse Core Ops, SparseCore 0:
  10.2 125.0 all-gather.2
